TPU v7x, 32 devices: a whole 2x2x4 slice. The times are simulated.
32 devices in a mesh: sp: 16 (over z, y, x), tp: 2 (over core).
Axes of the slice: x: 2, y: 2, z: 4, core: 2. Of those that a mesh axis runs over, the one named last changes fastest.
Arguments:
- stream_in: bfloat16 [4096, 2048], P('sp'), may hold values from -6 to 6
- norm_gain: float32 [2, 2048], replicated, may hold values from 0.1 to 1.9
- value_weight: bfloat16 [2, 2048, 2048], P(None, 'sp', 'tp'), may hold values from -0.125 to 0.125
- gate_weight: bfloat16 [2, 2048, 2048], P(None, 'sp', 'tp'), may hold values from -0.125 to 0.125
- conv_taps: float32 [2, 31, 2048], P(None, None, 'tp'), may hold values from -5 to 5
- channel_gain: float32 [2, 2048], P(None, 'tp'), may hold values from 0.1 to 1.9
- out_weight: bfloat16 [2, 2048, 2048], P(None, 'tp', 'sp'), may hold values from -0.125 to 0.125
Outputs:
- stream_out: bfloat16 [4096, 2048], P('sp')
All inputs are finite; a program needn't handle non-finite values.
Results may differ from a plain program's by a relative error of at most 0.015.
Values may be sent and summed in bfloat16 or wider, within the bound.
A program may use at most 64 MiB of HBM per device.

v0:
```python
import jax
import jax.numpy as jnp
from jax import lax
from jax.sharding import PartitionSpec as P

LAYERS = 2


epsilon = 1e-05


def passed_along(value, axis, steps):
    count = lax.axis_size(axis)
    leading, last = (max(0, -steps), min(count, count - steps))
    return lax.ppermute(value, axis, [(source, source + steps) for source in range(leading, last)])


def body(stream_in, norm_gain, value_weight, gate_weight, conv_taps, channel_gain, out_weight):
    stream = stream_in
    tok_rows = stream_in.shape[0]
    width = stream_in.shape[1]
    kernel = conv_taps.shape[1]
    local_cols = value_weight.shape[2]
    for layer in range(LAYERS):
        wide = stream.astype(jnp.float32)
        normed = (
            wide
            * lax.rsqrt(jnp.mean(wide * wide, axis=1, keepdims=True) + epsilon)
            * norm_gain[layer]
        ).astype(jnp.bfloat16)
        value = jnp.dot(
            normed,
            lax.all_gather(value_weight[layer], "sp", axis=0, tiled=True),
            preferred_element_type=jnp.float32,
        )
        gate = jnp.dot(
            normed,
            lax.all_gather(gate_weight[layer], "sp", axis=0, tiled=True),
            preferred_element_type=jnp.float32,
        )
        gated = (value * jax.nn.sigmoid(gate)).astype(jnp.bfloat16)
        earlier = passed_along(gated[tok_rows - (kernel - 1) :], "sp", 1)
        padded = jnp.concatenate([earlier, gated], axis=0).astype(jnp.float32)
        taps = conv_taps[layer]
        filtered = jnp.zeros((tok_rows, local_cols), jnp.float32)
        for tap in range(kernel):
            filtered = filtered + taps[tap] * padded[tap : tap + tok_rows]
        sum_first, sum_second = lax.psum(
            (jnp.sum(filtered, axis=1), jnp.sum(filtered * filtered, axis=1)), "tp"
        )
        mean_value = (sum_first / width)[:, None]
        variance = (sum_second / width)[:, None] - mean_value * mean_value
        activated = jax.nn.silu(
            (filtered - mean_value) * lax.rsqrt(variance + epsilon) * channel_gain[layer]
        ).astype(jnp.bfloat16)
        whole_out = lax.all_gather(out_weight[layer], "sp", axis=1, tiled=True)
        terms = jnp.dot(activated, whole_out, preferred_element_type=jnp.float32)
        summed = lax.psum(terms.astype(jnp.bfloat16), "tp").astype(jnp.float32)
        stream = (wide + summed).astype(jnp.bfloat16)
    return stream


def solution(mesh):
    return jax.shard_map(
        body,
        mesh=mesh,
        in_specs=(
            P("sp", None),
            P(),
            P(None, "sp", "tp"),
            P(None, "sp", "tp"),
            P(None, None, "tp"),
            P(None, "tp"),
            P(None, "tp", "sp"),
        ),
        out_specs=P("sp", None),
        check_vma=False,
    )
```

profile of v0, /device:TPU:0, one launch (start us, length us, event | category | flops | bytes accessed | tf_op | source)
XLA Modules:
  0.0 556.1 jit_solution(6253315192449355150)
XLA Ops:
  6.5 2.0 fusion.142
  8.5 0.0 all-gather.15.cloned.1.call-update
  8.6 0.0 all-gather.13.cloned.1.call-start
  8.6 1.9 fusion.141
  10.5 0.0 all-gather.13.cloned.1.call-update
  10.6 0.0 all-gather.17.cloned.1.call-start
  10.6 0.8 fusion.143
  11.4 0.0 all-gather.17.cloned.1.call-update
  11.5 0.0 all-reduce.5.cloned.1.call-start
  11.5 0.3 fusion.18
  11.9 0.1 fusion.146
  11.9 0.1 fusion.145
  12.0 76.4 %all-gather.15.cloned.1.call-done = bf16[1,2048,1024]{2,1,0:T(8,128)(2,1)} async-done(((bf16[1,128,1024]{2,1,0:T(8,128)(2,1)}), bf16[1,2048,1024]{2,1,0:T(8,128)(2,1)}) %all-gather.15.cloned.1.call-update) | async-done | bytes 4194320 | tf_op jit(solution)/shard_map/all_gather | solution.py:38
  88.5 3.6 fusion.56
  92.1 73.4 %all-gather.13.cloned.1.call-done = bf16[1,2048,1024]{2,1,0:T(8,128)(2,1)} async-done(((bf16[1,128,1024]{2,1,0:T(8,128)(2,1)}), bf16[1,2048,1024]{2,1,0:T(8,128)(2,1)}) %all-gather.13.cloned.1.call-update) | async-done | bytes 4194320 | tf_op jit(solution)/shard_map/all_gather | solution.py:33
  165.4 3.5 fusion.53
  169.0 3.4 collective-permute-start
  172.4 1.9 collective-permute-done
  174.2 0.2 maximum_convert_fusion
  174.4 5.8 %fusion.137 = (f32[256]{0:T(256)S(1)}, f32[256]{0:T(256)S(1)}, f32[256,1024]{1,0:T(8,128)S(1)}) fusion(f32[286,1024]{1,0:T(8,128)S(1)} %maximum_convert_fusion, f32[1024]{0:T(1024)S(1)} %bitcast.146, f32[1024]{0:T(1024)S(1)} %bitcast.147, f32[1024]{0:T(1024)S(1)} %bitcast.148, f32[1024]{0:T(1024)S(1)} %bitcast.149, f32[1024]{0:T(1024)S(1)} %bitcast.150, ...), kind=kLoop, calls=%fused_computation.185 | loop fusion | flops 16776704 | bytes 33683456 | tf_op jit(solution)/shard_map/reduce_sum | solution.py:49
  180.2 2.5 all-reduce.1
  182.7 72.8 %all-gather.17.cloned.1.call-done = bf16[1,1024,2048]{2,1,0:T(8,128)(2,1)} async-done(((bf16[1,1024,128]{2,1,0:T(8,128)(2,1)}), bf16[1,1024,2048]{2,1,0:T(8,128)(2,1)}) %all-gather.17.cloned.1.call-update) | async-done | bytes 4194320 | tf_op jit(solution)/shard_map/all_gather | solution.py:56
  255.5 4.7 fusion.12
  260.2 0.0 all-reduce.5.cloned.1.call-update
  260.2 0.0 all-gather.21.cloned.1.call-start
  260.3 0.5 all-gather.21.cloned.1.call-update
  260.8 0.0 all-gather.19.cloned.1.call-start
  260.9 0.5 all-gather.19.cloned.1.call-update
  261.4 0.0 all-gather.23.cloned.1.call-start
  261.4 0.7 all-gather.23.cloned.1.call-update
  262.1 0.0 all-reduce.7.cloned.1.call-start
  262.2 15.8 %all-reduce.5.cloned.1.call-done = bf16[256,2048]{1,0:T(8,128)(2,1)} async-done(((bf16[256,2048]{1,0:T(8,128)(2,1)}), bf16[256,2048]{1,0:T(8,128)(2,1)}) %all-reduce.5.cloned.1.call-update) | async-done | bytes 1048592 | tf_op jit(solution)/shard_map/psum | solution.py:58
  278.0 1.7 fusion.22
  279.7 77.7 %all-gather.21.cloned.1.call-done = bf16[1,2048,1024]{2,1,0:T(8,128)(2,1)} async-done(((bf16[1,128,1024]{2,1,0:T(8,128)(2,1)}), bf16[1,2048,1024]{2,1,0:T(8,128)(2,1)}) %all-gather.21.cloned.1.call-update) | async-done | bytes 4194320 | tf_op jit(solution)/shard_map/all_gather | solution.py:38
  357.4 3.6 fusion.59
  361.0 73.3 %all-gather.19.cloned.1.call-done = bf16[1,2048,1024]{2,1,0:T(8,128)(2,1)} async-done(((bf16[1,128,1024]{2,1,0:T(8,128)(2,1)}), bf16[1,2048,1024]{2,1,0:T(8,128)(2,1)}) %all-gather.19.cloned.1.call-update) | async-done | bytes 4194320 | tf_op jit(solution)/shard_map/all_gather | solution.py:33
  434.3 3.5 fusion.50
  437.8 3.5 collective-permute-start.1
  441.4 0.1 fusion.144
  441.5 1.6 collective-permute-done.1
  443.1 0.1 maximum_convert_fusion.1
  443.2 5.8 %fusion.136 = (f32[256]{0:T(256)S(1)}, f32[256]{0:T(256)S(1)}, f32[256,1024]{1,0:T(8,128)S(1)}) fusion(f32[286,1024]{1,0:T(8,128)S(1)} %maximum_convert_fusion.1, f32[1024]{0:T(1024)S(1)} %bitcast.112, f32[1024]{0:T(1024)S(1)} %bitcast.113, f32[1024]{0:T(1024)S(1)} %bitcast.156, f32[1024]{0:T(1024)S(1)} %bitcast.157, f32[1024]{0:T(1024)S(1)} %bitcast.158, ...), kind=kLoop, calls=%fused_computation.184 | loop fusion | flops 16776704 | bytes 33683456 | tf_op jit(solution)/shard_map/reduce_sum | solution.py:49
  449.1 2.5 all-reduce
  451.5 72.8 %all-gather.23.cloned.1.call-done = bf16[1,1024,2048]{2,1,0:T(8,128)(2,1)} async-done(((bf16[1,1024,128]{2,1,0:T(8,128)(2,1)}), bf16[1,1024,2048]{2,1,0:T(8,128)(2,1)}) %all-gather.23.cloned.1.call-update) | async-done | bytes 4194320 | tf_op jit(solution)/shard_map/all_gather | solution.py:56
  524.3 4.7 fusion.15
  529.0 0.0 all-reduce.7.cloned.1.call-update
  529.0 17.8 %all-reduce.7.cloned.1.call-done = bf16[256,2048]{1,0:T(8,128)(2,1)} async-done(((bf16[256,2048]{1,0:T(8,128)(2,1)}), bf16[256,2048]{1,0:T(8,128)(2,1)}) %all-reduce.7.cloned.1.call-update) | async-done | bytes 1048592 | tf_op jit(solution)/shard_map/psum | solution.py:58
  546.8 2.5 fusion.25
  (20 shorter events, 0.1 us)
Async XLA Ops:
  6.5 4.1 copy-start.1
  6.5 5.0 copy-start
  6.5 81.9 %all-gather.15.cloned.1.call-start = ((), (), s32[]{:S(2)}) async-start(), calls=%async_computation.3 | async-start | bytes 4456448 | tf_op jit(solution)/shard_map/all_gather | solution.py:38
  8.5 3.3 copy-start.2
  8.5 3.5 copy-start.3
  8.6 156.9 %all-gather.13.cloned.1.call-start = ((), (), s32[]{:S(2)}) async-start(), calls=%async_computation.2 | async-start | bytes 4456448 | tf_op jit(solution)/shard_map/all_gather | solution.py:33
  10.6 244.9 %all-gather.17.cloned.1.call-start = ((), (), s32[]{:S(2)}) async-start(), calls=%async_computation.4 | async-start | bytes 4456448 | tf_op jit(solution)/shard_map/all_gather | solution.py:56
  11.5 266.5 %all-reduce.5.cloned.1.call-start = ((), (), s32[]{:S(2)}) async-start(), calls=%async_computation | async-start | bytes 2097152 | tf_op jit(solution)/shard_map/psum | solution.py:58
  92.0 80.3 %copy-start.4 = (f32[2,1024]{1,0:T(2,128)S(1)}, f32[2,1024]{1,0:T(2,128)}, u32[]{:S(2)}) copy-start(f32[2,1024]{1,0:T(2,128)} %param.12) | copy-start | bytes 24580
  169.0 5.2 collective-permute-start
  260.2 97.2 %all-gather.21.cloned.1.call-start = ((), (), s32[]{:S(2)}) async-start(), calls=%async_computation.6 | async-start | bytes 4456448 | tf_op jit(solution)/shard_map/all_gather | solution.py:38
  260.8 173.5 %all-gather.19.cloned.1.call-start = ((), (), s32[]{:S(2)}) async-start(), calls=%async_computation.5 | async-start | bytes 4456448 | tf_op jit(solution)/shard_map/all_gather | solution.py:33
  261.4 262.9 %all-gather.23.cloned.1.call-start = ((), (), s32[]{:S(2)}) async-start(), calls=%async_computation.7 | async-start | bytes 4456448 | tf_op jit(solution)/shard_map/all_gather | solution.py:56
  262.1 284.6 %all-reduce.7.cloned.1.call-start = ((), (), s32[]{:S(2)}) async-start(), calls=%async_computation.1 | async-start | bytes 2097152 | tf_op jit(solution)/shard_map/psum | solution.py:58
  437.8 5.3 collective-permute-start.1
Sparse Core Ops, SparseCore 0:
  10.1 78.3 all-gather.14
  91.2 74.1 all-gather.12
  168.2 87.3 all-gather.16
  260.3 17.5 all-reduce.4
  280.6 76.7 all-gather.20
  360.0 74.1 all-gather.18
  437.0 87.3 all-gather.22
  529.1 17.5 all-reduce.6
where the time goes:
time: 557 us; the launch traced here: 556 us
  waiting for transfers between devices  485 us (87%)
  matrix products  23.6 us (4%)
  other arithmetic  16.5 us (3%)
  between operations  13.7 us (2%)
  starting transfers between devices  7.18 us (1%)
    all_gather x2, waiting for transfers between devices, body(): lax.all_gather(gate_weight[layer], 'sp', axis=0, tiled=True)  154 us
    all_gather x2, waiting for transfers between devices, body(): lax.all_gather(value_weight[layer], 'sp', axis=0, tiled=True)  147 us
    all_gather x2, waiting for transfers between devices, body(): whole_out = lax.all_gather(out_weight[layer], 'sp', axis=1, tiled=True)  146 us
    psum x2, waiting for transfers between devices, body(): summed = lax.psum(terms.astype(jnp.bfloat16), 'tp').astype(jnp.float32)  33.6 us
    reduce_sum x2, other arithmetic, body(): jnp.sum(filtered, axis=1)  11.6 us
  transfers between devices with their start and end apart: 10, of which 10 were waited for; matrix products, arithmetic and copies ran while one was open for 6% of the time, Pallas kernels for 0%

commit v1 on v0

v1 whole, which is shorter than its diff:
```python
import functools

import jax
import jax.numpy as jnp
from jax import lax
from jax.experimental import pallas as pl
from jax.experimental.pallas import tpu as pltpu
from jax.sharding import PartitionSpec as P

epsilon = 1e-05
MESH = pl.DeviceIdType.MESH
F32 = jnp.float32
BF16 = jnp.bfloat16
PAD = 32


def kernel(n, layers, taps_n, stream_in, gain, vw, gw, taps, cgain, ow, out,
           wv, wg, wo, nrm, gat, hsend, hrecv, fil, ssend, srecv, act,
           dsend, drecv, xsend, xrecv, strm,
           loc_sem, wx_send, wx_recv, ring_send, ring_recv, msg_send, msg_recv):
    ring = n // 2
    s = lax.axis_index("sp")
    c = lax.axis_index("tp")
    o, i = s // 2, s % 2
    toks, width = stream_in.shape
    group = 2 * toks
    rows, cols = vw.shape[1], vw.shape[2]
    ch = cols // 2
    half = width // 2

    def place(outer):
        z, y = outer // 2, outer % 2
        return (1 - y) * z + y * (ring - 1 - z)

    def outer_at(pos):
        h = pos // (ring // 2)
        return 2 * ((1 - h) * pos + h * (ring - 1 - pos)) + h

    p = place(o)
    nxt = outer_at((p + 1) % ring) * 2 + i
    prv = outer_at((p + ring - 1) % ring) * 2 + i
    mate = o * 2 + 1 - i
    up = ((o + 1) % ring) * 2 + i
    down = ((o + ring - 1) % ring) * 2 + i
    x_dev, d_dev, xd_dev = (mate, c), (s, 1 - c), (mate, 1 - c)

    barrier = pltpu.get_barrier_semaphore()
    everyone = [x_dev, d_dev, xd_dev, (nxt, c), (prv, c), (up, c), (down, c)]
    for dev in everyone:
        pl.semaphore_signal(barrier, inc=1, device_id=dev, device_id_type=MESH)
    pl.semaphore_wait(barrier, len(everyone))

    def al(v, m):
        return pl.multiple_of(v, m)

    my_rows = pl.ds(al(s * rows, rows), rows)
    my_cols = pl.ds(al(i * ch, ch), ch)
    mate_cols = pl.ds(al((1 - i) * ch, ch), ch)

    def weight_views(l, kind):
        if kind == 0:
            return vw.at[l, :, my_cols], vw.at[l, :, mate_cols], wv.at[l, my_rows, :]
        if kind == 1:
            return gw.at[l, :, my_cols], gw.at[l, :, mate_cols], wg.at[l, my_rows, :]
        return ow.at[l, my_cols, :], ow.at[l, mate_cols, :], wo.at[l, :, my_rows]

    local, crossed = {}, {}

    def start_local(l, kind):
        src, _, dst = weight_views(l, kind)
        local[l, kind] = pltpu.make_async_copy(src, dst, loc_sem.at[l * 3 + kind])
        local[l, kind].start()

    def start_cross(l, kind):
        _, src, dst = weight_views(l, kind)
        crossed[l, kind] = pltpu.make_async_remote_copy(
            src, dst, wx_send.at[l * 3 + kind], wx_recv.at[l * 3 + kind],
            device_id=x_dev, device_id_type=MESH)
        crossed[l, kind].start()

    pending = {}

    def chunk(l, grp, d, q, pos):
        src = outer_at(pos)
        if grp == 0:
            w = wv if d == 0 else wg
            return w.at[l, pl.ds(al((src * 2 + q) * rows, rows), rows), :]
        quarter = ch // 4
        return wo.at[l, pl.ds((d * 2 + q) * quarter, quarter),
                     pl.ds(al(src * 2 * rows, 2 * rows), 2 * rows)]

    ready = set()

    def own_ready(l, kind):
        if (l, kind) not in ready:
            ready.add((l, kind))
            local[l, kind].wait()
            crossed[l, kind].wait()

    def pump(l, grp, t):
        if t == 0:
            for kind in ((0, 1) if grp == 0 else (2,)):
                own_ready(l, kind)
        for q in range(2):
            for d in range(2):
                k = (l * 2 + grp) * 2 + d
                if t > 0:
                    pending[k, q].wait()
                if t < ring - 1:
                    pos = (p + ring - t) % ring if d == 0 else (p + t) % ring
                    ref = chunk(l, grp, d, q, pos)
                    pending[k, q] = pltpu.make_async_remote_copy(
                        ref, ref, ring_send.at[k, q], ring_recv.at[k, q, t],
                        device_id=(nxt if d == 0 else prv, c), device_id_type=MESH)
                    pending[k, q].start()

    queue = [(0, 1, t) for t in range(ring)]
    for l in range(1, layers):
        queue += [(l, 0, t) for t in range(ring)] + [(l, 1, t) for t in range(ring)]
    done = []

    def pumps(count):
        for _ in range(count):
            if queue:
                item = queue.pop(0)
                pump(*item)
                done.append(item)

    def finish(l, grp):
        while (l, grp, ring - 1) not in done:
            pumps(1)

    def message(slot, src, dst, dev):
        m = pltpu.make_async_remote_copy(src, dst, msg_send.at[slot], msg_recv.at[slot],
                                         device_id=dev, device_id_type=MESH)
        m.start()
        return m

    for l in range(layers):
        for kind in range(3):
            start_local(l, kind)
    start_cross(0, 0)
    start_cross(0, 1)

    own_tok = al(i * toks, toks)
    mate_tok = al((1 - i) * toks, toks)
    own_half = pl.ds(al(c * half, half), half)
    mate_half = pl.ds(al((1 - c) * half, half), half)
    tile = 128 if toks % 128 == 0 else toks
    per_layer = 8

    for l in range(layers):
        base = l * per_layer
        source = stream_in if l == 0 else strm.at[l - 1]

        def norm_step(r, _):
            at = al(r * 64, 64)
            wide = source[pl.ds(at, 64), :].astype(F32)
            scale = lax.rsqrt(jnp.mean(wide * wide, axis=1, keepdims=True) + epsilon)
            nrm[l, pl.ds(al(own_tok + at, 64), 64), :] = (wide * scale * gain[l:l + 1, :]).astype(BF16)
            return 0

        lax.fori_loop(0, toks // 64, norm_step, 0)
        spot = nrm.at[l, pl.ds(own_tok, toks), own_half]
        got = nrm.at[l, pl.ds(mate_tok, toks), own_half]
        gather = message(base + 0, spot, spot, x_dev)
        if l == 0:
            start_cross(0, 2)
            for ll in range(1, layers):
                for kind in range(3):
                    start_cross(ll, kind)
            for t in range(ring - 2):
                pump(0, 0, t)
            gather.wait()
            relay = message(base + 1, got, got, d_dev)
            pump(0, 0, ring - 2)
            pumps(1)
            pump(0, 0, ring - 1)
            pumps(1)
        else:
            pumps(3)
            gather.wait()
            relay = message(base + 1, got, got, d_dev)
            finish(l, 0)
        relay.wait()

        def gate_step(r, _):
            at = al(r * tile, tile)
            x = nrm[l, pl.ds(at, tile), :]
            value = jnp.dot(x, wv[l], preferred_element_type=F32)
            gate = jnp.dot(x, wg[l], preferred_element_type=F32)
            gated = (value * jax.nn.sigmoid(gate)).astype(BF16)
            gat[pl.ds(al(PAD + at, 32), tile), :] = gated.astype(F32)
            return 0

        lax.fori_loop(0, group // tile, gate_step, 0)
        hsend[l] = gat[group:group + PAD, :].astype(BF16)
        halo = message(base + 2, hsend.at[l], hrecv.at[l], (up, c))
        pumps(1)
        halo.wait()
        first = (o > 0).astype(F32)
        gat[0:PAD, :] = hrecv[l].astype(F32) * first

        lead = PAD - (taps_n - 1)
        step_rows = 64
        lanes = 128

        def conv_step(r, _):
            at = al(r * step_rows, step_rows)
            for lane in range(ch // lanes):
                cut = slice(lane * lanes, (lane + 1) * lanes)
                total = jnp.zeros((step_rows, lanes), F32)
                block = gat[pl.ds(at, step_rows + PAD), cut]
                for b in range(8):
                    moved = block if b == 0 else pltpu.roll(block, step_rows + PAD - b, 0)
                    for a in range(PAD // 8 + 1):
                        tap = 8 * a + b - lead
                        if 0 <= tap < taps_n:
                            total = total + taps[l, tap:tap + 1, cut] * moved[8 * a:8 * a + step_rows]
                fil[pl.ds(at, step_rows), cut] = total
            return 0

        parts = 2
        per = group // step_rows // parts
        for part in range(parts):
            lax.fori_loop(part * per, (part + 1) * per, conv_step, 0)
            pumps(1)

        wide = fil[...]
        first_sum = jnp.sum(wide, axis=1, keepdims=True)
        second_sum = jnp.sum(wide * wide, axis=1, keepdims=True)
        lane_id = lax.broadcasted_iota(jnp.int32, (group, lanes), 1)
        stat = jnp.where(lane_id == 0, first_sum, jnp.where(lane_id == 1, second_sum, 0.0))
        ssend[l] = jnp.transpose(stat)[0:8, :]
        sums = [message(base + 3 + k, ssend.at[l], srecv.at[l, k], dev)
                for k, dev in enumerate((x_dev, d_dev, xd_dev))]
        pumps(1)
        for m in sums:
            m.wait()
        whole = ssend[l] + srecv[l, 0] + srecv[l, 1] + srecv[l, 2]
        stat = jnp.transpose(jnp.concatenate([whole] + [jnp.zeros((lanes - 8, group), F32)], axis=0))
        mean_value = stat[:, 0:1] / width
        variance = stat[:, 1:2] / width - mean_value * mean_value
        act[...] = jax.nn.silu((fil[...] - mean_value) * lax.rsqrt(variance + epsilon)
                               * cgain[l:l + 1, pl.ds(al(i * ch, ch), ch)]).astype(BF16)
        finish(l, 1)

        def other_step(r, _):
            at = al(r * tile, tile)
            dsend[l, pl.ds(at, tile), :] = jnp.dot(
                act[pl.ds(at, tile), :], wo[l, :, mate_half], preferred_element_type=F32).astype(BF16)
            return 0

        lax.fori_loop(0, group // tile, other_step, 0)
        swap = message(base + 6, dsend.at[l], drecv.at[l], d_dev)
        swap.wait()

        def mate_step(r, _):
            at = al(mate_tok + r * tile, tile)
            mine = jnp.dot(act[pl.ds(at, tile), :], wo[l, :, own_half], preferred_element_type=F32)
            xsend[l, pl.ds(al(r * tile, tile), tile), :] = (
                mine + drecv[l, pl.ds(at, tile), :].astype(F32)).astype(BF16)
            return 0

        lax.fori_loop(0, toks // tile, mate_step, 0)
        scatter = message(base + 7, xsend.at[l], xrecv.at[l], x_dev)
        pumps(2)
        scatter.wait()

        def own_step(r, _):
            at = al(own_tok + r * tile, tile)
            here = pl.ds(al(r * tile, tile), tile)
            mine = jnp.dot(act[pl.ds(at, tile), :], wo[l, :, own_half], preferred_element_type=F32)
            branch = mine + drecv[l, pl.ds(at, tile), :].astype(F32) + xrecv[l, here, :].astype(F32)
            strm[l, here, own_half] = (source[here, own_half].astype(F32) + branch).astype(BF16)
            return 0

        lax.fori_loop(0, toks // tile, own_step, 0)
        piece = strm.at[l, :, own_half]
        message(layers * per_layer + l, piece, piece, d_dev).wait()

    out[...] = strm[layers - 1]


def fused(n, layers):
    def body(stream_in, norm_gain, value_weight, gate_weight, conv_taps, channel_gain, out_weight):
        toks, width = stream_in.shape
        taps_n = conv_taps.shape[1]
        rows, cols = value_weight.shape[1], value_weight.shape[2]
        ch, half, group, ring = cols // 2, width // 2, 2 * toks, n // 2
        i = lax.axis_index("sp") % 2
        taps = lax.dynamic_slice_in_dim(conv_taps, i * ch, ch, axis=2)
        vmem = pl.BlockSpec(memory_space=pltpu.VMEM)
        hbm = pl.BlockSpec(memory_space=pltpu.HBM)
        msgs = layers * 9
        return pl.pallas_call(
            functools.partial(kernel, n, layers, taps_n),
            out_shape=jax.ShapeDtypeStruct((toks, width), BF16),
            in_specs=[vmem, vmem, hbm, hbm, vmem, vmem, hbm],
            out_specs=vmem,
            scratch_shapes=[
                pltpu.VMEM((layers, width, ch), BF16),
                pltpu.VMEM((layers, width, ch), BF16),
                pltpu.VMEM((layers, ch, width), BF16),
                pltpu.VMEM((layers, group, width), BF16),
                pltpu.VMEM((PAD + group, ch), F32),
                pltpu.VMEM((layers, PAD, ch), BF16),
                pltpu.VMEM((layers, PAD, ch), BF16),
                pltpu.VMEM((group, ch), F32),
                pltpu.VMEM((layers, 8, group), F32),
                pltpu.VMEM((layers, 3, 8, group), F32),
                pltpu.VMEM((group, ch), BF16),
                pltpu.VMEM((layers, group, half), BF16),
                pltpu.VMEM((layers, group, half), BF16),
                pltpu.VMEM((layers, toks, half), BF16),
                pltpu.VMEM((layers, toks, half), BF16),
                pltpu.VMEM((layers, toks, width), BF16),
                pltpu.SemaphoreType.DMA((layers * 3,)),
                pltpu.SemaphoreType.DMA((layers * 3,)),
                pltpu.SemaphoreType.DMA((layers * 3,)),
                pltpu.SemaphoreType.DMA((layers * 4, 2)),
                pltpu.SemaphoreType.DMA((layers * 4, 2, ring - 1)),
                pltpu.SemaphoreType.DMA((msgs,)),
                pltpu.SemaphoreType.DMA((msgs,)),
            ],
            compiler_params=pltpu.CompilerParams(
                collective_id=0, has_side_effects=True, vmem_limit_bytes=62 * 2**20),
        )(stream_in, norm_gain, value_weight, gate_weight, taps, channel_gain, out_weight)

    return body


def passed_along(value, axis, steps):
    count = lax.axis_size(axis)
    leading, last = (max(0, -steps), min(count, count - steps))
    return lax.ppermute(value, axis, [(source, source + steps) for source in range(leading, last)])


def general(stream_in, norm_gain, value_weight, gate_weight, conv_taps, channel_gain, out_weight):
    stream = stream_in
    tok_rows = stream_in.shape[0]
    width = stream_in.shape[1]
    taps_n = conv_taps.shape[1]
    local_cols = value_weight.shape[2]
    for layer in range(norm_gain.shape[0]):
        wide = stream.astype(F32)
        normed = (
            wide
            * lax.rsqrt(jnp.mean(wide * wide, axis=1, keepdims=True) + epsilon)
            * norm_gain[layer]
        ).astype(BF16)
        value = jnp.dot(normed, lax.all_gather(value_weight[layer], "sp", axis=0, tiled=True),
                        preferred_element_type=F32)
        gate = jnp.dot(normed, lax.all_gather(gate_weight[layer], "sp", axis=0, tiled=True),
                       preferred_element_type=F32)
        gated = (value * jax.nn.sigmoid(gate)).astype(BF16)
        earlier = passed_along(gated[tok_rows - (taps_n - 1):], "sp", 1)
        padded = jnp.concatenate([earlier, gated], axis=0).astype(F32)
        taps = conv_taps[layer]
        filtered = jnp.zeros((tok_rows, local_cols), F32)
        for tap in range(taps_n):
            filtered = filtered + taps[tap] * padded[tap:tap + tok_rows]
        sum_first, sum_second = lax.psum(
            (jnp.sum(filtered, axis=1), jnp.sum(filtered * filtered, axis=1)), "tp")
        mean_value = (sum_first / width)[:, None]
        variance = (sum_second / width)[:, None] - mean_value * mean_value
        activated = jax.nn.silu(
            (filtered - mean_value) * lax.rsqrt(variance + epsilon) * channel_gain[layer]
        ).astype(BF16)
        whole_out = lax.all_gather(out_weight[layer], "sp", axis=1, tiled=True)
        terms = jnp.dot(activated, whole_out, preferred_element_type=F32)
        summed = lax.psum(terms.astype(BF16), "tp").astype(F32)
        stream = (wide + summed).astype(BF16)
    return stream


def solution(mesh):
    n, tp = mesh.shape["sp"], mesh.shape["tp"]

    def body(stream_in, norm_gain, value_weight, *rest):
        rows, cols = value_weight.shape[1], value_weight.shape[2]
        pairs = tp == 2 and n % 4 == 0 and rows % 128 == 0 and cols % 1024 == 0
        fits = stream_in.shape[0] % 64 == 0 and rest[1].shape[1] <= PAD
        chosen = fused(n, norm_gain.shape[0]) if pairs and fits else general
        return chosen(stream_in, norm_gain, value_weight, *rest)

    return jax.shard_map(
        body,
        mesh=mesh,
        in_specs=(
            P("sp", None),
            P(),
            P(None, "sp", "tp"),
            P(None, "sp", "tp"),
            P(None, None, "tp"),
            P(None, "tp"),
            P(None, "tp", "sp"),
        ),
        out_specs=P("sp", None),
        check_vma=False,
    )
```

time: 557 us -> 193 us (0.35)
  waiting for transfers between devices: 485 us -> 0 us
  Pallas kernels: 0 us -> 189 us
  matrix products: 23.6 us -> 0 us
  other arithmetic: 16.5 us -> 0 us
  between operations: 13.7 us -> 0.01 us
  starting transfers between devices: 7.18 us -> 0 us
    all_gather x6 -> x0, waiting for transfers between devices: 446 us -> none  [the longest x2 154 us: body(): lax.all_gather(gate_weight[layer], 'sp', axis=0, tiled=True)]
    pallas_call x0 -> x1, Pallas kernels: none -> 189 us  [body(): pl.pallas_call(functools.partial(kernel, n, layers, taps_n), out_shape=ja...]
    psum x2 -> x0, waiting for transfers between devices: 33.6 us -> none  [body(): summed = lax.psum(terms.astype(jnp.bfloat16), 'tp').astype(jnp.float32)]
    dot_general x6 -> x0, matrix products: 23.6 us -> none  [the longest x2 9.38 us: body(): terms = jnp.dot(activated, whole_out, preferred_element_type=jnp.float32)]
    reduce_sum x4 -> x0, other arithmetic: 13.6 us -> none  [the longest x2 11.6 us: body(): jnp.sum(filtered, axis=1)]
    ppermute x2 -> x0, starting transfers between devices: 6.9 us -> none  [passed_along(): lax.ppermute(value, axis, [(source, source + steps) for source in range(l...]
  transfers between devices with their start and end apart: 10 -> 0, of which waited for: 10 -> 0; matrix products, arithmetic and copies ran while one was open for 6% -> 0% of each run, Pallas kernels for 0% -> 0%
where the time goes in v1:
time: 193 us; the launch traced here: 192 us
  Pallas kernels  189 us (98%)
  local copies, waits for them, and re-layouts  3.94 us (2%)
    pallas_call x1, Pallas kernels, body(): pl.pallas_call(functools.partial(kernel, n, layers, taps_n), out_shape=ja...  189 us
    unnamed x4, local copies, waits for them, and re-layouts  3.93 us

profile of v1, /device:TPU:0, one launch (start us, length us, event | category | flops | bytes accessed | tf_op | source)
XLA Modules:
  0.0 192.5 jit_solution(1327142312660864322)
XLA Ops:
  0.0 0.0 copy-start
  0.0 0.9 copy-done
  1.0 0.7 copy.9.taps
  1.6 188.5 %shard_map.73 = bf16[256,2048]{1,0:T(8,128)(2,1)} custom-call(bf16[256,2048]{1,0:T(8,128)(2,1)} %stream_in.1, f32[2,2048]{1,0:T(2,128)} %gain.1, bf16[2,128,1024]{2,1,0:T(8,128)(2,1)} %vw.1, bf16[2,128,1024]{2,1,0:T(8,128)(2,1)} %gw.1, f32[2,31,512]{2,1,0:T(8,128)} %copy.9.taps, f32[2,1024]{1,0:T(2,128)} %cgain.1, bf16[2,1024,128]{2,1,0:T(8,128)(2,1)} %ow.1), custom_call_target="tpu_custom_call" | custom-call | tf_op jit(solution)/shard_map/pallas_call | solution.py:296
  190.2 2.3 %copy.11 = bf16[256,2048]{1,0:T(8,128)(2,1)} copy(bf16[256,2048]{1,0:T(8,128)(2,1)} %shard_map.73) | data formatting | bytes 2097152
  (1 shorter events, 0.0 us)
Async XLA Ops:
  0.0 0.9 copy-start

commit v2 on v1

--- a/solution.py
+++ b/solution.py
@@ -12,11 +12,13 @@
 F32 = jnp.float32
 BF16 = jnp.bfloat16
 PAD = 32
+EARLY = 3
+SPLIT = 1
 
 
 def kernel(n, layers, taps_n, stream_in, gain, vw, gw, taps, cgain, ow, out,
            wv, wg, wo, nrm, gat, hsend, hrecv, fil, ssend, srecv, act,
-           dsend, drecv, xsend, xrecv, strm,
+           dsend, drecv, xsend, xrecv, strm, keep,
            loc_sem, wx_send, wx_recv, ring_send, ring_recv, msg_send, msg_recv):
     ring = n // 2
     s = lax.axis_index("sp")
@@ -80,28 +82,29 @@
 
     pending = {}
 
+    def block_cols(pos, d):
+        return pl.ds(al((outer_at(pos) * 2 + d) * rows, rows), rows)
+
     def chunk(l, grp, d, q, pos):
-        src = outer_at(pos)
         if grp == 0:
-            w = wv if d == 0 else wg
-            return w.at[l, pl.ds(al((src * 2 + q) * rows, rows), rows), :]
-        quarter = ch // 4
-        return wo.at[l, pl.ds((d * 2 + q) * quarter, quarter),
-                     pl.ds(al(src * 2 * rows, 2 * rows), 2 * rows)]
-
-    ready = set()
-
-    def own_ready(l, kind):
-        if (l, kind) not in ready:
-            ready.add((l, kind))
-            local[l, kind].wait()
-            crossed[l, kind].wait()
+            block = outer_at(pos) * 2 + (i + q // SPLIT) % 2
+            w, size = (wv if d == 0 else wg), rows // SPLIT
+            return w.at[l, pl.ds(al(block * rows + q % SPLIT * size, size), size), :]
+        size = ch // 2 // SPLIT
+        return wo.at[l, pl.ds(q * size, size), block_cols(pos, d)]
+
+    def own_ready(l, grp, q):
+        if grp == 0 and q % SPLIT == 0:
+            for kind in (0, 1):
+                (crossed if q else local)[l, kind].wait()
+        if grp == 1 and q == 0:
+            local[l, 2].wait()
+            crossed[l, 2].wait()
 
     def pump(l, grp, t):
-        if t == 0:
-            for kind in ((0, 1) if grp == 0 else (2,)):
-                own_ready(l, kind)
-        for q in range(2):
+        for q in range(2 * SPLIT):
+            if t == 0:
+                own_ready(l, grp, q)
             for d in range(2):
                 k = (l * 2 + grp) * 2 + d
                 if t > 0:
@@ -114,9 +117,19 @@
                         device_id=(nxt if d == 0 else prv, c), device_id_type=MESH)
                     pending[k, q].start()
 
-    queue = [(0, 1, t) for t in range(ring)]
-    for l in range(1, layers):
-        queue += [(l, 0, t) for t in range(ring)] + [(l, 1, t) for t in range(ring)]
+    queue = []
+    for l in range(layers):
+        main = [(l, 0, t) for t in range(1 if l else 0, ring)]
+        side = [(l, 1, t) for t in range(ring)]
+        early = min(EARLY, ring)
+        queue += main[:len(main) - early]
+        for t in range(early):
+            queue += [main[len(main) - early + t], side[t]]
+        rest = side[early:]
+        queue += rest[:len(rest) // 2]
+        if l + 1 < layers:
+            queue.append((l + 1, 0, 0))
+        queue += rest[len(rest) // 2:]
     done = []
 
     def pumps(count):
@@ -126,8 +139,8 @@
                 pump(*item)
                 done.append(item)
 
-    def finish(l, grp):
-        while (l, grp, ring - 1) not in done:
+    def ensure(l, grp, t):
+        while (l, grp, t) not in done:
             pumps(1)
 
     def message(slot, src, dst, dev):
@@ -145,9 +158,8 @@
     own_tok = al(i * toks, toks)
     mate_tok = al((1 - i) * toks, toks)
     own_half = pl.ds(al(c * half, half), half)
-    mate_half = pl.ds(al((1 - c) * half, half), half)
     tile = 128 if toks % 128 == 0 else toks
-    per_layer = 8
+    per_layer = 6 + ring * 3
 
     for l in range(layers):
         base = l * per_layer
@@ -169,19 +181,12 @@
             for ll in range(1, layers):
                 for kind in range(3):
                     start_cross(ll, kind)
-            for t in range(ring - 2):
-                pump(0, 0, t)
-            gather.wait()
-            relay = message(base + 1, got, got, d_dev)
-            pump(0, 0, ring - 2)
-            pumps(1)
-            pump(0, 0, ring - 1)
-            pumps(1)
+            pumps(3)
         else:
-            pumps(3)
-            gather.wait()
-            relay = message(base + 1, got, got, d_dev)
-            finish(l, 0)
+            pumps(2)
+        gather.wait()
+        relay = message(base + 1, got, got, d_dev)
+        ensure(l, 0, ring - 1)
         relay.wait()
 
         def gate_step(r, _):
@@ -243,41 +248,48 @@
         variance = stat[:, 1:2] / width - mean_value * mean_value
         act[...] = jax.nn.silu((fil[...] - mean_value) * lax.rsqrt(variance + epsilon)
                                * cgain[l:l + 1, pl.ds(al(i * ch, ch), ch)]).astype(BF16)
-        finish(l, 1)
-
-        def other_step(r, _):
-            at = al(r * tile, tile)
-            dsend[l, pl.ds(at, tile), :] = jnp.dot(
-                act[pl.ds(at, tile), :], wo[l, :, mate_half], preferred_element_type=F32).astype(BF16)
-            return 0
-
-        lax.fori_loop(0, group // tile, other_step, 0)
-        swap = message(base + 6, dsend.at[l], drecv.at[l], d_dev)
-        swap.wait()
-
-        def mate_step(r, _):
-            at = al(mate_tok + r * tile, tile)
-            mine = jnp.dot(act[pl.ds(at, tile), :], wo[l, :, own_half], preferred_element_type=F32)
-            xsend[l, pl.ds(al(r * tile, tile), tile), :] = (
-                mine + drecv[l, pl.ds(at, tile), :].astype(F32)).astype(BF16)
-            return 0
-
-        lax.fori_loop(0, toks // tile, mate_step, 0)
-        scatter = message(base + 7, xsend.at[l], xrecv.at[l], x_dev)
-        pumps(2)
-        scatter.wait()
-
-        def own_step(r, _):
-            at = al(own_tok + r * tile, tile)
-            here = pl.ds(al(r * tile, tile), tile)
-            mine = jnp.dot(act[pl.ds(at, tile), :], wo[l, :, own_half], preferred_element_type=F32)
-            branch = mine + drecv[l, pl.ds(at, tile), :].astype(F32) + xrecv[l, here, :].astype(F32)
-            strm[l, here, own_half] = (source[here, own_half].astype(F32) + branch).astype(BF16)
-            return 0
-
-        lax.fori_loop(0, toks // tile, own_step, 0)
-        piece = strm.at[l, :, own_half]
-        message(layers * per_layer + l, piece, piece, d_dev).wait()
+
+        slot = base + 6
+        own_rows, mate_rows = pl.ds(own_tok, toks), pl.ds(mate_tok, toks)
+        swaps, scatters, lasts = [], [], []
+
+        def own_block(u):
+            return block_cols((p + ring + (2 * c - 1) * u) % ring, c)
+
+        def stage_swap(u):
+            columns = block_cols((p + ring + (1 - 2 * c) * u) % ring, 1 - c)
+            dsend[l, u] = jnp.dot(act[...], wo[l, :, columns], preferred_element_type=F32).astype(BF16)
+            swaps.append(message(slot + u, dsend.at[l, u], drecv.at[l, u], d_dev))
+
+        def stage_scatter(u):
+            weights = wo[l, :, own_block(u)]
+            away = jnp.dot(act[mate_rows, :], weights, preferred_element_type=F32)
+            mine = jnp.dot(act[own_rows, :], weights, preferred_element_type=F32)
+            swaps[u].wait()
+            xsend[l, u] = (away + drecv[l, u, mate_rows, :].astype(F32)).astype(BF16)
+            scatters.append(message(slot + ring + u, xsend.at[l, u], xrecv.at[l, u], x_dev))
+            keep[u] = (mine + drecv[l, u, own_rows, :].astype(F32)
+                       + source[:, own_block(u)].astype(F32))
+
+        def stage_last(u):
+            scatters[u].wait()
+            strm[l, :, own_block(u)] = (keep[u] + xrecv[l, u].astype(F32)).astype(BF16)
+            piece = strm.at[l, :, own_block(u)]
+            lasts.append(message(slot + 2 * ring + u, piece, piece, d_dev))
+
+        lag = 2
+        for u in range(ring + 1 + lag):
+            if u < ring:
+                ensure(l, 1, u)
+                stage_swap(u)
+            if 1 <= u <= ring:
+                stage_scatter(u - 1)
+            if u % 3 == 1:
+                pumps(1 if l + 1 < layers else 0)
+            if u >= 1 + lag:
+                stage_last(u - 1 - lag)
+        for m in lasts:
+            m.wait()
 
     out[...] = strm[layers - 1]
 
@@ -292,7 +304,7 @@
         taps = lax.dynamic_slice_in_dim(conv_taps, i * ch, ch, axis=2)
         vmem = pl.BlockSpec(memory_space=pltpu.VMEM)
         hbm = pl.BlockSpec(memory_space=pltpu.HBM)
-        msgs = layers * 9
+        msgs = layers * (6 + ring * 3)
         return pl.pallas_call(
             functools.partial(kernel, n, layers, taps_n),
             out_shape=jax.ShapeDtypeStruct((toks, width), BF16),
@@ -310,16 +322,17 @@
                 pltpu.VMEM((layers, 8, group), F32),
                 pltpu.VMEM((layers, 3, 8, group), F32),
                 pltpu.VMEM((group, ch), BF16),
-                pltpu.VMEM((layers, group, half), BF16),
-                pltpu.VMEM((layers, group, half), BF16),
-                pltpu.VMEM((layers, toks, half), BF16),
-                pltpu.VMEM((layers, toks, half), BF16),
+                pltpu.VMEM((layers, ring, group, rows), BF16),
+                pltpu.VMEM((layers, ring, group, rows), BF16),
+                pltpu.VMEM((layers, ring, toks, rows), BF16),
+                pltpu.VMEM((layers, ring, toks, rows), BF16),
                 pltpu.VMEM((layers, toks, width), BF16),
+                pltpu.VMEM((ring, toks, rows), F32),
                 pltpu.SemaphoreType.DMA((layers * 3,)),
                 pltpu.SemaphoreType.DMA((layers * 3,)),
                 pltpu.SemaphoreType.DMA((layers * 3,)),
-                pltpu.SemaphoreType.DMA((layers * 4, 2)),
-                pltpu.SemaphoreType.DMA((layers * 4, 2, ring - 1)),
+                pltpu.SemaphoreType.DMA((layers * 4, 2 * SPLIT)),
+                pltpu.SemaphoreType.DMA((layers * 4, 2 * SPLIT, ring - 1)),
                 pltpu.SemaphoreType.DMA((msgs,)),
                 pltpu.SemaphoreType.DMA((msgs,)),
             ],

time: 193 us -> 169 us (0.88)
  Pallas kernels: 189 us -> 165 us
    pallas_call x1, Pallas kernels: 189 us -> 165 us  [body(): pl.pallas_call(functools.partial(kernel, n, layers, taps_n), out_shape=ja...]
where the time goes in v2:
time: 169 us; the launch traced here: 168 us
  Pallas kernels  165 us (98%)
  local copies, waits for them, and re-layouts  3.94 us (2%)
    pallas_call x1, Pallas kernels, body(): pl.pallas_call(functools.partial(kernel, n, layers, taps_n), out_shape=ja...  165 us
    unnamed x4, local copies, waits for them, and re-layouts  3.93 us

profile of v2, /device:TPU:0, one launch (start us, length us, event | category | flops | bytes accessed | tf_op | source)
XLA Modules:
  0.0 168.5 jit_solution(16661693525024363845)
XLA Ops:
  0.0 0.0 copy-start
  0.0 0.9 copy-done
  1.0 0.7 copy.9.taps
  1.6 164.5 %shard_map.73 = bf16[256,2048]{1,0:T(8,128)(2,1)} custom-call(bf16[256,2048]{1,0:T(8,128)(2,1)} %stream_in.1, f32[2,2048]{1,0:T(2,128)} %gain.1, bf16[2,128,1024]{2,1,0:T(8,128)(2,1)} %vw.1, bf16[2,128,1024]{2,1,0:T(8,128)(2,1)} %gw.1, f32[2,31,512]{2,1,0:T(8,128)} %copy.9.taps, f32[2,1024]{1,0:T(2,128)} %cgain.1, bf16[2,1024,128]{2,1,0:T(8,128)(2,1)} %ow.1), custom_call_target="tpu_custom_call" | custom-call | tf_op jit(solution)/shard_map/pallas_call | solution.py:308
  166.2 2.3 %copy.11 = bf16[256,2048]{1,0:T(8,128)(2,1)} copy(bf16[256,2048]{1,0:T(8,128)(2,1)} %shard_map.73) | data formatting | bytes 2097152
  (1 shorter events, 0.0 us)
Async XLA Ops:
  0.0 0.9 copy-start

commit v3 on v2

--- a/solution.py
+++ b/solution.py
@@ -12,7 +12,7 @@
 F32 = jnp.float32
 BF16 = jnp.bfloat16
 PAD = 32
-EARLY = 3
+EARLY, EARLY_LAST = 3, 2
 SPLIT = 1
 
 
@@ -121,7 +121,7 @@
     for l in range(layers):
         main = [(l, 0, t) for t in range(1 if l else 0, ring)]
         side = [(l, 1, t) for t in range(ring)]
-        early = min(EARLY, ring)
+        early = min(EARLY if l + 1 < layers else EARLY_LAST, ring)
         queue += main[:len(main) - early]
         for t in range(early):
             queue += [main[len(main) - early + t], side[t]]
@@ -183,7 +183,7 @@
                     start_cross(ll, kind)
             pumps(3)
         else:
-            pumps(2)
+            pumps(4)
         gather.wait()
         relay = message(base + 1, got, got, d_dev)
         ensure(l, 0, ring - 1)

time: 169 us -> 167 us (0.988)
  Pallas kernels: 165 us -> 163 us
    pallas_call x1, Pallas kernels: 165 us -> 163 us  [body(): pl.pallas_call(functools.partial(kernel, n, layers, taps_n), out_shape=ja...]
where the time goes in v3:
time: 167 us; the launch traced here: 166 us
  Pallas kernels  163 us (98%)
  local copies, waits for them, and re-layouts  3.94 us (2%)
    pallas_call x1, Pallas kernels, body(): pl.pallas_call(functools.partial(kernel, n, layers, taps_n), out_shape=ja...  163 us
    unnamed x4, local copies, waits for them, and re-layouts  3.93 us

profile of v3, /device:TPU:0, one launch (start us, length us, event | category | flops | bytes accessed | tf_op | source)
XLA Modules:
  0.0 166.5 jit_solution(16971570380511530538)
XLA Ops:
  0.0 0.0 copy-start
  0.0 0.9 copy-done
  1.0 0.7 copy.9.taps
  1.6 162.5 %shard_map.73 = bf16[256,2048]{1,0:T(8,128)(2,1)} custom-call(bf16[256,2048]{1,0:T(8,128)(2,1)} %stream_in.1, f32[2,2048]{1,0:T(2,128)} %gain.1, bf16[2,128,1024]{2,1,0:T(8,128)(2,1)} %vw.1, bf16[2,128,1024]{2,1,0:T(8,128)(2,1)} %gw.1, f32[2,31,512]{2,1,0:T(8,128)} %copy.9.taps, f32[2,1024]{1,0:T(2,128)} %cgain.1, bf16[2,1024,128]{2,1,0:T(8,128)(2,1)} %ow.1), custom_call_target="tpu_custom_call" | custom-call | tf_op jit(solution)/shard_map/pallas_call | solution.py:308
  164.2 2.3 %copy.11 = bf16[256,2048]{1,0:T(8,128)(2,1)} copy(bf16[256,2048]{1,0:T(8,128)(2,1)} %shard_map.73) | data formatting | bytes 2097152
  (1 shorter events, 0.0 us)
Async XLA Ops:
  0.0 0.9 copy-start
